TPU v7x, 32 devices: a whole 2x2x4 slice. The times are simulated.
32 devices in a mesh: fs: 8 (over z, y), tp: 4 (over x, core).
Axes of the slice: x: 2, y: 2, z: 4, core: 2. Of those that a mesh axis runs over, the one named last changes fastest.
Arguments:
- weights_in: float32 [2, 2048, 5632], P(None, 'fs', 'tp'), may hold values from -6 to 6
- weights_mix: float32 [2048, 2048], P('fs', 'tp'), may hold values from -6 to 6
- momentum_in: float32 [2, 2048, 5632], P(None, 'fs', 'tp'), may hold values from -5 to 5
- momentum_mix: float32 [2048, 2048], P('fs', 'tp'), may hold values from -5 to 5
- grads_in: float32 [2, 2048, 5632], P(None, 'fs', 'tp'), may hold values from -5 to 5
- grads_mix: float32 [2048, 2048], P('fs', 'tp'), may hold values from -5 to 5
Outputs:
- momentum_in_next: float32 [2, 2048, 5632], P(None, 'fs', 'tp')
- momentum_mix_next: float32 [2048, 2048], P('fs', 'tp')
- weights_in_next: float32 [2, 2048, 5632], P(None, 'fs', 'tp')
- weights_mix_next: float32 [2048, 2048], P('fs', 'tp')
- update_in: float32 [2, 2048, 5632], P(None, 'fs', 'tp')
- update_mix: float32 [2048, 2048], P('fs', 'tp')
All inputs are finite; a program needn't handle non-finite values.
Results may differ from a plain program's by a relative error of at most 0.0003.
Values sent between devices are 32-bit elements; how exact they have to be, the bound alone decides.
A program may use at most 128 MiB of HBM per device.

v0:
```python
import math
import jax
import jax.numpy as jnp
from jax import lax
from jax.sharding import PartitionSpec as P

D = 2048
FF = 5632
ITERS = 3
A_COEF = 3.4445
B_COEF = -4.775
C_COEF = 2.0315
MOMENTUM_DECAY = 0.95
STEP_RATE = 0.02
HIGH = lax.Precision.HIGHEST


def row_squares(shard):
    return jnp.sum(jnp.square(shard), axis=(1, 2))


def scale_from(summed):
    return (0.5 * lax.rsqrt(jnp.maximum(summed / D, 1.0)))[:, None, None]


def local(weights_in, weights_mix, momentum_in, momentum_mix, grads_in, grads_mix):
    moment_in = MOMENTUM_DECAY * momentum_in + grads_in
    moment_mix = MOMENTUM_DECAY * momentum_mix + grads_mix
    local_in = moment_in
    local_mix = moment_mix[None]
    squares = jnp.concatenate([row_squares(local_in), row_squares(local_mix)])
    scaling = scale_from(lax.psum(squares, ("fs", "tp")))
    for iteration in range(ITERS):
        cols_in, cols_mix = (
            lax.all_gather(local_in, "fs", axis=1, tiled=True),
            lax.all_gather(local_mix, "fs", axis=1, tiled=True),
        )
        partial_value = jnp.concatenate(
            [
                jnp.einsum("krc,ksc->krs", local_in, cols_in, precision=HIGH),
                jnp.einsum("krc,ksc->krs", local_mix, cols_mix, precision=HIGH),
            ]
        )
        gram_block = lax.psum_scatter(partial_value, "tp", scatter_dimension=2, tiled=True)
        gram_rows = lax.all_gather(gram_block, "tp", axis=2, tiled=True)
        factor = scaling if iteration == 0 else jnp.ones_like(scaling)
        gram_cols = lax.all_gather(gram_block, "fs", axis=1, tiled=True)
        square = jnp.einsum("krs,ksc->krc", gram_rows, gram_cols, precision=HIGH)
        poly_mat = factor**2 * B_COEF * gram_block + factor**4 * C_COEF * square
        poly_rows = lax.all_gather(poly_mat, "tp", axis=2, tiled=True)
        local_in = factor[:2] * (
            A_COEF * local_in + jnp.einsum("krs,ksc->krc", poly_rows[:2], cols_in, precision=HIGH)
        )
        local_mix = factor[2:] * (
            A_COEF * local_mix + jnp.einsum("krs,ksc->krc", poly_rows[2:], cols_mix, precision=HIGH)
        )
    step_in = local_in * math.sqrt(max(D, FF))
    step_mix = local_mix[0] * math.sqrt(D)
    return (
        moment_in,
        moment_mix,
        weights_in - STEP_RATE * step_in,
        weights_mix - STEP_RATE * step_mix,
        step_in,
        step_mix,
    )


def solution(mesh):
    in_specs = (
        P(None, "fs", "tp"),
        P("fs", "tp"),
        P(None, "fs", "tp"),
        P("fs", "tp"),
        P(None, "fs", "tp"),
        P("fs", "tp"),
    )
    out_specs = (
        P(None, "fs", "tp"),
        P("fs", "tp"),
        P(None, "fs", "tp"),
        P("fs", "tp"),
        P(None, "fs", "tp"),
        P("fs", "tp"),
    )
    return jax.shard_map(local, mesh=mesh, in_specs=in_specs, out_specs=out_specs, check_vma=False)
```

profile of v0, /device:TPU:0, one launch (start us, length us, event | category | flops | bytes accessed | tf_op | source)
XLA Modules:
  0.0 2754.7 jit_solution(12206210918786785973)
XLA Ops:
  7.2 0.0 all-gather.43.cloned.1.call-start
  7.2 2.7 multiply_reduce_fusion.1
  9.9 0.0 all-gather.43.cloned.1.call-update
  9.9 0.0 all-gather.19.cloned.1.call-start
  10.0 4.7 multiply_reduce_fusion
  14.7 0.0 all-gather.19.cloned.1.call-update
  14.7 0.0 reduce-scatter.4.cloned.1.call-start
  14.7 71.5 %all-gather.43.cloned.1.call-done = f32[2048,512]{1,0:T(8,128)} async-done(((f32[256,512]{1,0:T(8,128)}), f32[2048,512]{1,0:T(8,128)}) %all-gather.43.cloned.1.call-update) | async-done | bytes 4194320 | tf_op jit(solution)/shard_map/all_gather | solution.py:36
  86.2 7.1 convolution_bitcast_fusion.2
  93.4 434.6 %all-gather.19.cloned.1.call-done = f32[2,2048,1408]{2,1,0:T(8,128)} async-done(((f32[2,256,1408]{2,1,0:T(8,128)}), f32[2,2048,1408]{2,1,0:T(8,128)}) %all-gather.19.cloned.1.call-update) | async-done | bytes 23068688 | tf_op jit(solution)/shard_map/all_gather | solution.py:35
  528.0 24.5 fusion.8
  552.5 3.1 pad_maximum_fusion
  555.6 0.0 all-gather.21.cloned.1.call-start
  555.7 58.0 %reduce-scatter.4.cloned.1.call-done = f32[3,256,512]{2,1,0:T(8,128)} async-done(((f32[3,256,2048]{2,1,0:T(8,128)}), f32[3,256,512]{2,1,0:T(8,128)}) %reduce-scatter.4.cloned.1.call-update) | async-done | bytes 1572880 | tf_op jit(solution)/shard_map/reduce_scatter | solution.py:44
  613.7 0.0 all-gather.23.cloned.1.call-start
  613.7 0.5 all-gather.23.cloned.1.call-update
  614.3 0.0 all-gather.25.cloned.1.call-start
  614.3 0.7 pad_maximum_fusion.3
  615.0 40.5 %psum.7 = f32[3]{0:T(128)S(1)} all-reduce(f32[3]{0:T(128)S(1)} %pad_maximum_fusion.3), channel_id=1, replica_groups=mesh['fs'=8,'tp'=4] {'fs','tp'}, use_global_device_ids=true, to_apply=%region_2.0 | all-reduce | flops 3 | bytes 24 | tf_op jit(solution)/shard_map/psum | solution.py:32
  655.6 6.8 all-gather.21.cloned.1.call-done
  662.3 178.2 %all-gather.23.cloned.1.call-done = f32[3,2048,512]{2,1,0:T(8,128)} async-done(((f32[3,256,512]{2,1,0:T(8,128)}), f32[3,2048,512]{2,1,0:T(8,128)}) %all-gather.23.cloned.1.call-update) | async-done | bytes 12582928 | tf_op jit(solution)/shard_map/all_gather | solution.py:47
  840.5 17.5 multiply_add_fusion.3
  858.0 0.0 all-gather.45.cloned.1.call-start
  858.1 0.6 slice.28
  858.7 44.1 %all-gather.25.cloned.1.call-done = f32[3,256,2048]{2,1,0:T(8,128)} async-done(((f32[3,256,512]{2,1,0:T(8,128)}), f32[3,256,2048]{2,1,0:T(8,128)}) %all-gather.25.cloned.1.call-update) | async-done | bytes 6291472 | tf_op jit(solution)/shard_map/all_gather | solution.py:50
  902.7 8.0 fusion.5
  910.7 0.6 all-gather.27.cloned.1.call-start
  911.3 27.5 fusion
  938.8 0.2 reduce-scatter.6.cloned.1.call-start
  939.0 44.6 %all-gather.45.cloned.1.call-done = f32[2048,512]{1,0:T(8,128)} async-done(((f32[256,512]{1,0:T(8,128)}), f32[2048,512]{1,0:T(8,128)}) %all-gather.45.cloned.1.call-update) | async-done | bytes 4194320 | tf_op jit(solution)/shard_map/all_gather | solution.py:36
  983.7 7.1 convolution_bitcast_fusion.1
  990.8 434.6 %all-gather.27.cloned.1.call-done = f32[2,2048,1408]{2,1,0:T(8,128)} async-done(((f32[2,256,1408]{2,1,0:T(8,128)}), f32[2,2048,1408]{2,1,0:T(8,128)}) %all-gather.27.cloned.1.call-update) | async-done | bytes 23068688 | tf_op jit(solution)/shard_map/all_gather | solution.py:35
  1425.4 24.5 fusion.9
  1449.9 3.1 pad_maximum_fusion.1
  1453.1 0.0 all-gather.29.cloned.1.call-start
  1453.1 58.0 %reduce-scatter.6.cloned.1.call-done = f32[3,256,512]{2,1,0:T(8,128)} async-done(((f32[3,256,2048]{2,1,0:T(8,128)}), f32[3,256,512]{2,1,0:T(8,128)}) %reduce-scatter.6.cloned.1.call-update) | async-done | bytes 1572880 | tf_op jit(solution)/shard_map/reduce_scatter | solution.py:44
  1511.1 0.0 all-gather.31.cloned.1.call-start
  1511.2 0.7 all-gather.31.cloned.1.call-update
  1511.9 0.3 all-gather.33.cloned.1.call-start
  1512.1 46.8 %all-gather.29.cloned.1.call-done = f32[3,256,2048]{2,1,0:T(8,128)} async-done(((f32[3,256,512]{2,1,0:T(8,128)}), f32[3,256,2048]{2,1,0:T(8,128)}) %all-gather.29.cloned.1.call-update) | async-done | bytes 6291472 | tf_op jit(solution)/shard_map/all_gather | solution.py:45
  1558.9 178.3 %all-gather.31.cloned.1.call-done = f32[3,2048,512]{2,1,0:T(8,128)} async-done(((f32[3,256,512]{2,1,0:T(8,128)}), f32[3,2048,512]{2,1,0:T(8,128)}) %all-gather.31.cloned.1.call-update) | async-done | bytes 12582928 | tf_op jit(solution)/shard_map/all_gather | solution.py:47
  1737.2 17.5 multiply_add_fusion.2
  1754.8 0.0 all-gather.47.cloned.1.call-start
  1754.8 44.6 %all-gather.33.cloned.1.call-done = f32[3,256,2048]{2,1,0:T(8,128)} async-done(((f32[3,256,512]{2,1,0:T(8,128)}), f32[3,256,2048]{2,1,0:T(8,128)}) %all-gather.33.cloned.1.call-update) | async-done | bytes 6291472 | tf_op jit(solution)/shard_map/all_gather | solution.py:50
  1799.5 7.3 fusion.6
  1806.8 0.3 all-gather.35.cloned.1.call-start
  1807.1 27.4 convolution_add_fusion.1
  1834.5 0.5 reduce-scatter.8.cloned.1.call-start
  1835.0 44.7 %all-gather.47.cloned.1.call-done = f32[2048,512]{1,0:T(8,128)} async-done(((f32[256,512]{1,0:T(8,128)}), f32[2048,512]{1,0:T(8,128)}) %all-gather.47.cloned.1.call-update) | async-done | bytes 4194320 | tf_op jit(solution)/shard_map/all_gather | solution.py:36
  1879.7 7.1 convolution_bitcast_fusion
  1886.9 434.4 %all-gather.35.cloned.1.call-done = f32[2,2048,1408]{2,1,0:T(8,128)} async-done(((f32[2,256,1408]{2,1,0:T(8,128)}), f32[2,2048,1408]{2,1,0:T(8,128)}) %all-gather.35.cloned.1.call-update) | async-done | bytes 23068688 | tf_op jit(solution)/shard_map/all_gather | solution.py:35
  2321.3 24.5 fusion.10
  2345.9 3.1 pad_maximum_fusion.2
  2349.0 0.0 all-gather.37.cloned.1.call-start
  2349.1 58.0 %reduce-scatter.8.cloned.1.call-done = f32[3,256,512]{2,1,0:T(8,128)} async-done(((f32[3,256,2048]{2,1,0:T(8,128)}), f32[3,256,512]{2,1,0:T(8,128)}) %reduce-scatter.8.cloned.1.call-update) | async-done | bytes 1572880 | tf_op jit(solution)/shard_map/reduce_scatter | solution.py:44
  2407.0 0.0 all-gather.39.cloned.1.call-start
  2407.1 0.5 all-gather.39.cloned.1.call-update
  2407.6 0.2 all-gather.41.cloned.1.call-start
  2407.9 47.0 %all-gather.37.cloned.1.call-done = f32[3,256,2048]{2,1,0:T(8,128)} async-done(((f32[3,256,512]{2,1,0:T(8,128)}), f32[3,256,2048]{2,1,0:T(8,128)}) %all-gather.37.cloned.1.call-update) | async-done | bytes 6291472 | tf_op jit(solution)/shard_map/all_gather | solution.py:45
  2454.8 178.2 %all-gather.39.cloned.1.call-done = f32[3,2048,512]{2,1,0:T(8,128)} async-done(((f32[3,256,512]{2,1,0:T(8,128)}), f32[3,2048,512]{2,1,0:T(8,128)}) %all-gather.39.cloned.1.call-update) | async-done | bytes 12582928 | tf_op jit(solution)/shard_map/all_gather | solution.py:47
  2633.0 17.5 multiply_add_fusion.1
  2650.5 44.7 %all-gather.41.cloned.1.call-done = f32[3,256,2048]{2,1,0:T(8,128)} async-done(((f32[3,256,512]{2,1,0:T(8,128)}), f32[3,256,2048]{2,1,0:T(8,128)}) %all-gather.41.cloned.1.call-update) | async-done | bytes 6291472 | tf_op jit(solution)/shard_map/all_gather | solution.py:50
  2695.2 46.1 %broadcast_multiply_fusion = (f32[2,256,1408]{2,1,0:T(8,128)}, f32[2,256,1408]{2,1,0:T(8,128)}) fusion(f32[2,256,1408]{2,1,0:T(8,128)} %param.6, f32[3,256,2048]{2,1,0:T(8,128)} %all-gather.41.cloned.1.call-done, f32[2,2048,1408]{2,1,0:T(8,128)} %all-gather.35.cloned.1.call-done, f32[2,256,1408]{2,1,0:T(8,128)S(1)} %copy-done.2), kind=kOutput, calls=%fused_computation.22 | convolution fusion | flops 17720344576 | bytes 40894464 | tf_op jit(solution)/shard_map/krs,ksc->krc/dot_general | solution.py:52
  2741.3 6.3 broadcast_multiply_fusion.1
  (37 shorter events, 0.3 us)
Async XLA Ops:
  7.2 79.1 %all-gather.43.cloned.1.call-start = ((), (), s32[]{:S(2)}) async-start(), calls=%async_computation.18 | async-start | bytes 4718592 | tf_op jit(solution)/shard_map/all_gather | solution.py:36
  9.9 76.3 %copy-start.9 = (f32[256,512]{1,0:T(8,128)S(1)}, f32[256,512]{1,0:T(8,128)}, u32[]{:S(2)}) copy-start(f32[256,512]{1,0:T(8,128)} %get-tuple-element.11) | copy-start | bytes 1572868
  9.9 518.0 %all-gather.19.cloned.1.call-start = ((), (), s32[]{:S(2)}) async-start(), calls=%async_computation.3 | async-start | bytes 25952256 | tf_op jit(solution)/shard_map/all_gather | solution.py:35
  14.7 513.3 %copy-start = (f32[2,256,1408]{2,1,0:T(8,128)S(1)}, f32[2,256,1408]{2,1,0:T(8,128)}, u32[]{:S(2)}) copy-start(f32[2,256,1408]{2,1,0:T(8,128)} %get-tuple-element.9) | copy-start | bytes 8650756
  14.7 599.0 %reduce-scatter.4.cloned.1.call-start = ((), (), s32[]{:S(2)}) async-start(), calls=%async_computation.4 | async-start | bytes 7864320 | tf_op jit(solution)/shard_map/reduce_scatter | solution.py:44
  528.0 24.6 copy-start.6
  555.6 106.7 %all-gather.21.cloned.1.call-start = ((), (), s32[]{:S(2)}) async-start(), calls=%async_computation.5 | async-start | bytes 7864320 | tf_op jit(solution)/shard_map/all_gather | solution.py:45
  613.7 226.8 %all-gather.23.cloned.1.call-start = ((), (), s32[]{:S(2)}) async-start(), calls=%async_computation.6 | async-start | bytes 14155776 | tf_op jit(solution)/shard_map/all_gather | solution.py:47
  614.3 288.5 %all-gather.25.cloned.1.call-start = ((), (), s32[]{:S(2)}) async-start(), calls=%async_computation.7 | async-start | bytes 7864320 | tf_op jit(solution)/shard_map/all_gather | solution.py:50
  858.0 125.6 %all-gather.45.cloned.1.call-start = ((), (), s32[]{:S(2)}) async-start(), calls=%async_computation.19 | async-start | bytes 4718592 | tf_op jit(solution)/shard_map/all_gather | solution.py:36
  910.7 514.7 %all-gather.27.cloned.1.call-start = ((), (), s32[]{:S(2)}) async-start(), calls=%async_computation.8 | async-start | bytes 25952256 | tf_op jit(solution)/shard_map/all_gather | solution.py:35
  911.3 72.4 %copy-start.5 = (f32[256,512]{1,0:T(8,128)S(1)}, f32[256,512]{1,0:T(8,128)}, u32[]{:S(2)}) copy-start(f32[256,512]{1,0:T(8,128)} %fusion.5) | copy-start | bytes 1572868
  938.8 486.6 %copy-start.1 = (f32[2,256,1408]{2,1,0:T(8,128)S(1)}, f32[2,256,1408]{2,1,0:T(8,128)}, u32[]{:S(2)}) copy-start(f32[2,256,1408]{2,1,0:T(8,128)} %fusion) | copy-start | bytes 8650756
  938.8 572.3 %reduce-scatter.6.cloned.1.call-start = ((), (), s32[]{:S(2)}) async-start(), calls=%async_computation.9 | async-start | bytes 7864320 | tf_op jit(solution)/shard_map/reduce_scatter | solution.py:44
  1425.4 24.6 copy-start.7
  1453.1 105.8 %all-gather.29.cloned.1.call-start = ((), (), s32[]{:S(2)}) async-start(), calls=%async_computation.10 | async-start | bytes 7864320 | tf_op jit(solution)/shard_map/all_gather | solution.py:45
  1511.1 226.1 %all-gather.31.cloned.1.call-start = ((), (), s32[]{:S(2)}) async-start(), calls=%async_computation.11 | async-start | bytes 14155776 | tf_op jit(solution)/shard_map/all_gather | solution.py:47
  1511.9 287.6 %all-gather.33.cloned.1.call-start = ((), (), s32[]{:S(2)}) async-start(), calls=%async_computation.12 | async-start | bytes 7864320 | tf_op jit(solution)/shard_map/all_gather | solution.py:50
  1754.8 125.0 %all-gather.47.cloned.1.call-start = ((), (), s32[]{:S(2)}) async-start(), calls=%async_computation.20 | async-start | bytes 4718592 | tf_op jit(solution)/shard_map/all_gather | solution.py:36
  1806.8 73.0 %copy-start.4 = (f32[256,512]{1,0:T(8,128)S(1)}, f32[256,512]{1,0:T(8,128)}, u32[]{:S(2)}) copy-start(f32[256,512]{1,0:T(8,128)} %fusion.6) | copy-start | bytes 1572868
  1806.8 514.5 %all-gather.35.cloned.1.call-start = ((), (), s32[]{:S(2)}) async-start(), calls=%async_computation.13 | async-start | bytes 25952256 | tf_op jit(solution)/shard_map/all_gather | solution.py:35
  1834.5 486.8 %copy-start.2 = (f32[2,256,1408]{2,1,0:T(8,128)S(1)}, f32[2,256,1408]{2,1,0:T(8,128)}, u32[]{:S(2)}) copy-start(f32[2,256,1408]{2,1,0:T(8,128)} %convolution_add_fusion.1) | copy-start | bytes 8650756
  1834.5 572.5 %reduce-scatter.8.cloned.1.call-start = ((), (), s32[]{:S(2)}) async-start(), calls=%async_computation.14 | async-start | bytes 7864320 | tf_op jit(solution)/shard_map/reduce_scatter | solution.py:44
  2321.3 24.6 copy-start.8
  2349.0 105.8 %all-gather.37.cloned.1.call-start = ((), (), s32[]{:S(2)}) async-start(), calls=%async_computation.15 | async-start | bytes 7864320 | tf_op jit(solution)/shard_map/all_gather | solution.py:45
  2407.0 225.9 %all-gather.39.cloned.1.call-start = ((), (), s32[]{:S(2)}) async-start(), calls=%async_computation.16 | async-start | bytes 14155776 | tf_op jit(solution)/shard_map/all_gather | solution.py:47
  2407.6 287.6 %all-gather.41.cloned.1.call-start = ((), (), s32[]{:S(2)}) async-start(), calls=%async_computation.17 | async-start | bytes 7864320 | tf_op jit(solution)/shard_map/all_gather | solution.py:50
  2695.2 46.1 %copy-start.3 = (f32[2048,512]{1,0:T(8,128)S(1)}, f32[2048,512]{1,0:T(8,128)}, u32[]{:S(2)}) copy-start(f32[2048,512]{1,0:T(8,128)} %all-gather.47.cloned.1.call-done) | copy-start | bytes 12582916
  2695.2 46.1 %copy-start.10 = (f32[256,512]{1,0:T(8,128)S(1)}, f32[256,512]{1,0:T(8,128)}, u32[]{:S(2)}) copy-start(f32[256,512]{1,0:T(8,128)} %param.7) | copy-start | bytes 1572868
Sparse Core Ops, SparseCore 0:
  10.7 75.5 all-gather.42
  88.3 439.5 all-gather.18
  555.8 57.8 reduce-scatter.3
  615.1 47.2 all-gather.20
  664.4 176.0 all-gather.22
  858.2 44.5 all-gather.24
  910.8 72.7 all-gather.44
  985.8 439.5 all-gather.26
  1453.2 57.8 reduce-scatter.5
  1512.5 46.3 all-gather.28
  1561.1 176.0 all-gather.30
  1754.9 44.5 all-gather.32
  1806.9 72.7 all-gather.46
  1881.7 439.5 all-gather.34
  2349.1 57.8 reduce-scatter.7
  2408.4 46.3 all-gather.36
  2456.8 176.0 all-gather.38
  2650.7 44.5 all-gather.40
where the time goes:
time: 2760 us; the launch traced here: 2750 us
  waiting for transfers between devices  2410 us (87%)
  matrix products  270 us (10%)
  blocking collectives  40.5 us (1%)
    all_gather x3, waiting for transfers between devices, local(): lax.all_gather(local_in, 'fs', axis=1, tiled=True)  1300 us
    all_gather x3, waiting for transfers between devices, local(): gram_cols = lax.all_gather(gram_block, 'fs', axis=1, tiled=True)  535 us
    reduce_scatter x3, waiting for transfers between devices, local(): lax.psum_scatter(partial_value, 'tp', scatter_dimension=2, tiled=True)  174 us
    all_gather x3, waiting for transfers between devices, local(): lax.all_gather(local_mix, 'fs', axis=1, tiled=True)  161 us
    all_gather x3, waiting for transfers between devices, local(): poly_rows = lax.all_gather(poly_mat, 'tp', axis=2, tiled=True)  133 us
    dot_general x3, matrix products, local(): jnp.einsum('krs,ksc->krc', poly_rows[:2], cols_in, precision=HIGH)  101 us
    all_gather x3, waiting for transfers between devices, local(): gram_rows = lax.all_gather(gram_block, 'tp', axis=2, tiled=True)  100 us
    dot_general x3, matrix products, local(): jnp.einsum('krc,ksc->krs', local_in, cols_in, precision=HIGH)  73.6 us
  transfers between devices with their start and end apart: 18, of which 18 were waited for; matrix products, arithmetic and copies ran while one was open for 3% of the time, Pallas kernels for 0%

commit v1 on v0

--- a/solution.py
+++ b/solution.py
@@ -44,8 +44,27 @@
         gram_block = lax.psum_scatter(partial_value, "tp", scatter_dimension=2, tiled=True)
         gram_rows = lax.all_gather(gram_block, "tp", axis=2, tiled=True)
         factor = scaling if iteration == 0 else jnp.ones_like(scaling)
-        gram_cols = lax.all_gather(gram_block, "fs", axis=1, tiled=True)
-        square = jnp.einsum("krs,ksc->krc", gram_rows, gram_cols, precision=HIGH)
+        size, position = (lax.axis_size("fs"), lax.axis_index("fs"))
+        left = [(i, (i - 1) % size) for i in range(size)]
+        rows = gram_block.shape[1]
+        current = gram_block
+        total = jnp.einsum(
+            "krs,ksc->krc",
+            lax.dynamic_slice_in_dim(gram_rows, position * rows, current.shape[1], axis=2),
+            current,
+            precision=HIGH,
+        )
+        for step in range(1, size):
+            current = lax.ppermute(current, "fs", left)
+            total = total + jnp.einsum(
+                "krs,ksc->krc",
+                lax.dynamic_slice_in_dim(
+                    gram_rows, (position + step) % size * rows, current.shape[1], axis=2
+                ),
+                current,
+                precision=HIGH,
+            )
+        square = total
         poly_mat = factor**2 * B_COEF * gram_block + factor**4 * C_COEF * square
         poly_rows = lax.all_gather(poly_mat, "tp", axis=2, tiled=True)
         local_in = factor[:2] * (

time: 2760 us -> 2850 us (1.033)
  starting transfers between devices: 2.52 us -> 106 us
  waiting for transfers between devices: 2410 us -> 2360 us
    ppermute x0 -> x21, waiting for transfers between devices: none -> 579 us  [local(): current = lax.ppermute(current, 'fs', left)]
    all_gather x3 -> x0, waiting for transfers between devices: 535 us -> none  [local(): gram_cols = lax.all_gather(gram_block, 'fs', axis=1, tiled=True)]
    ppermute x0 -> x21, starting transfers between devices: none -> 104 us  [local(): current = lax.ppermute(current, 'fs', left)]
    all_gather x3, waiting for transfers between devices: 100 us -> 0.02 us  [local(): gram_rows = lax.all_gather(gram_block, 'tp', axis=2, tiled=True)]
    dot_general x3 -> x24, matrix products: 52.6 us -> 63.2 us  [the longest x21 56.4 us: local(): jnp.einsum('krs,ksc->krc', lax.dynamic_slice_in_dim(gram_rows, (position...]
  transfers between devices with their start and end apart: 18 -> 36, of which waited for: 18 -> 32; matrix products, arithmetic and copies ran while one was open for 3% -> 5% of each run, Pallas kernels for 0% -> 0%
where the time goes in v1:
time: 2850 us
  waiting for transfers between devices  2360 us (83%)
  matrix products  272 us (10%)
  starting transfers between devices  106 us (4%)
  blocking collectives  63.7 us (2%)
    all_gather x3, waiting for transfers between devices, local(): lax.all_gather(local_in, 'fs', axis=1, tiled=True)  1300 us
    ppermute x21, waiting for transfers between devices, local(): current = lax.ppermute(current, 'fs', left)  579 us
    reduce_scatter x3, waiting for transfers between devices, local(): lax.psum_scatter(partial_value, 'tp', scatter_dimension=2, tiled=True)  174 us
    all_gather x3, waiting for transfers between devices, local(): lax.all_gather(local_mix, 'fs', axis=1, tiled=True)  162 us
    all_gather x3, waiting for transfers between devices, local(): poly_rows = lax.all_gather(poly_mat, 'tp', axis=2, tiled=True)  142 us
    ppermute x21, starting transfers between devices, local(): current = lax.ppermute(current, 'fs', left)  104 us
    dot_general x3, matrix products, local(): jnp.einsum('krs,ksc->krc', poly_rows[:2], cols_in, precision=HIGH)  89.9 us
    dot_general x3, matrix products, local(): jnp.einsum('krc,ksc->krs', local_in, cols_in, precision=HIGH)  73.6 us
  transfers between devices with their start and end apart: 36, of which 32 were waited for; matrix products, arithmetic and copies ran while one was open for 5% of the time, Pallas kernels for 0%

profile of v1, /device:TPU:0, one launch (start us, length us, event | category | flops | bytes accessed | tf_op | source)
XLA Modules:
  0.0 2846.2 jit_solution(2088919258547041636)
XLA Ops:
  14.7 71.5 %all-gather.34.cloned.1.call-done = f32[2048,512]{1,0:T(8,128)} async-done(((f32[256,512]{1,0:T(8,128)}), f32[2048,512]{1,0:T(8,128)}) %all-gather.34.cloned.1.call-update) | async-done | bytes 4194320 | tf_op jit(solution)/shard_map/all_gather | solution.py:36
  86.2 7.3 convolution_bitcast_fusion.2
  93.5 434.4 %all-gather.16.cloned.1.call-done = f32[2,2048,1408]{2,1,0:T(8,128)} async-done(((f32[2,256,1408]{2,1,0:T(8,128)}), f32[2,2048,1408]{2,1,0:T(8,128)}) %all-gather.16.cloned.1.call-update) | async-done | bytes 23068688 | tf_op jit(solution)/shard_map/all_gather | solution.py:35
  528.0 24.5 fusion.77
  555.8 58.0 %reduce-scatter.4.cloned.1.call-done = f32[3,256,512]{2,1,0:T(8,128)} async-done(((f32[3,256,2048]{2,1,0:T(8,128)}), f32[3,256,512]{2,1,0:T(8,128)}) %reduce-scatter.4.cloned.1.call-update) | async-done | bytes 1572880 | tf_op jit(solution)/shard_map/reduce_scatter | solution.py:44
  618.1 33.8 %collective-permute-done = f32[3,256,512]{2,1,0:T(8,128)S(1)} collective-permute-done((f32[3,256,512]{2,1,0:T(8,128)}, f32[3,256,512]{2,1,0:T(8,128)S(1)}, u32[]{:S(2)}, u32[]{:S(2)}) %collective-permute-start) | collective-permute-done | bytes 1572896 | tf_op jit(solution)/shard_map/ppermute | solution.py:58
  651.9 5.1 collective-permute-start.1
  656.9 32.6 %collective-permute-done.1 = f32[3,256,512]{2,1,0:T(8,128)S(1)} collective-permute-done((f32[3,256,512]{2,1,0:T(8,128)S(1)}, f32[3,256,512]{2,1,0:T(8,128)S(1)}, u32[]{:S(2)}, u32[]{:S(2)}) %collective-permute-start.1) | collective-permute-done | bytes 1572896 | tf_op jit(solution)/shard_map/ppermute | solution.py:58
  690.7 5.2 collective-permute-start.2
  695.9 31.8 %collective-permute-done.2 = f32[3,256,512]{2,1,0:T(8,128)S(1)} collective-permute-done((f32[3,256,512]{2,1,0:T(8,128)S(1)}, f32[3,256,512]{2,1,0:T(8,128)S(1)}, u32[]{:S(2)}, u32[]{:S(2)}) %collective-permute-start.2) | collective-permute-done | bytes 1572896 | tf_op jit(solution)/shard_map/ppermute | solution.py:58
  727.7 5.2 collective-permute-start.3
  732.9 30.9 %collective-permute-done.3 = f32[3,256,512]{2,1,0:T(8,128)S(1)} collective-permute-done((f32[3,256,512]{2,1,0:T(8,128)S(1)}, f32[3,256,512]{2,1,0:T(8,128)S(1)}, u32[]{:S(2)}, u32[]{:S(2)}) %collective-permute-start.3) | collective-permute-done | bytes 1572896 | tf_op jit(solution)/shard_map/ppermute | solution.py:58
  764.9 5.2 collective-permute-start.4
  770.1 30.1 %collective-permute-done.4 = f32[3,256,512]{2,1,0:T(8,128)} collective-permute-done((f32[3,256,512]{2,1,0:T(8,128)S(1)}, f32[3,256,512]{2,1,0:T(8,128)}, u32[]{:S(2)}, u32[]{:S(2)}) %collective-permute-start.4) | collective-permute-done | bytes 1572896 | tf_op jit(solution)/shard_map/ppermute | solution.py:58
  800.2 5.3 collective-permute-start.5
  806.2 63.7 %psum.7 = f32[3]{0:T(128)S(1)} all-reduce(f32[3]{0:T(128)S(1)} %pad_maximum_fusion.3), channel_id=1, replica_groups=mesh['fs'=8,'tp'=4] {'fs','tp'}, use_global_device_ids=true, to_apply=%region_2.0 | all-reduce | flops 3 | bytes 24 | tf_op jit(solution)/shard_map/psum | solution.py:32
  890.4 18.5 collective-permute-done.6
  913.3 47.2 %all-gather.20.cloned.1.call-done = f32[3,256,2048]{2,1,0:T(8,128)} async-done(((f32[3,256,512]{2,1,0:T(8,128)}), f32[3,256,2048]{2,1,0:T(8,128)}) %all-gather.20.cloned.1.call-update) | async-done | bytes 6291472 | tf_op jit(solution)/shard_map/all_gather | solution.py:69
  960.4 8.0 fusion.5
  968.5 27.4 fusion
  996.2 45.2 %all-gather.36.cloned.1.call-done = f32[2048,512]{1,0:T(8,128)} async-done(((f32[256,512]{1,0:T(8,128)}), f32[2048,512]{1,0:T(8,128)}) %all-gather.36.cloned.1.call-update) | async-done | bytes 4194320 | tf_op jit(solution)/shard_map/all_gather | solution.py:36
  1041.4 7.3 convolution_bitcast_fusion.1
  1048.7 434.4 %all-gather.22.cloned.1.call-done = f32[2,2048,1408]{2,1,0:T(8,128)} async-done(((f32[2,256,1408]{2,1,0:T(8,128)}), f32[2,2048,1408]{2,1,0:T(8,128)}) %all-gather.22.cloned.1.call-update) | async-done | bytes 23068688 | tf_op jit(solution)/shard_map/all_gather | solution.py:35
  1483.1 24.6 fusion.78
  1510.9 58.0 %reduce-scatter.6.cloned.1.call-done = f32[3,256,512]{2,1,0:T(8,128)} async-done(((f32[3,256,2048]{2,1,0:T(8,128)}), f32[3,256,512]{2,1,0:T(8,128)}) %reduce-scatter.6.cloned.1.call-update) | async-done | bytes 1572880 | tf_op jit(solution)/shard_map/reduce_scatter | solution.py:44
  1573.2 33.7 %collective-permute-done.7 = f32[3,256,512]{2,1,0:T(8,128)} collective-permute-done((f32[3,256,512]{2,1,0:T(8,128)}, f32[3,256,512]{2,1,0:T(8,128)}, u32[]{:S(2)}, u32[]{:S(2)}) %collective-permute-start.7) | collective-permute-done | bytes 1572896 | tf_op jit(solution)/shard_map/ppermute | solution.py:58
  1606.9 5.2 collective-permute-start.8
  1612.1 32.9 %collective-permute-done.8 = f32[3,256,512]{2,1,0:T(8,128)S(1)} collective-permute-done((f32[3,256,512]{2,1,0:T(8,128)}, f32[3,256,512]{2,1,0:T(8,128)S(1)}, u32[]{:S(2)}, u32[]{:S(2)}) %collective-permute-start.8) | collective-permute-done | bytes 1572896 | tf_op jit(solution)/shard_map/ppermute | solution.py:58
  1646.2 5.1 collective-permute-start.9
  1651.3 31.8 %collective-permute-done.9 = f32[3,256,512]{2,1,0:T(8,128)S(1)} collective-permute-done((f32[3,256,512]{2,1,0:T(8,128)S(1)}, f32[3,256,512]{2,1,0:T(8,128)S(1)}, u32[]{:S(2)}, u32[]{:S(2)}) %collective-permute-start.9) | collective-permute-done | bytes 1572896 | tf_op jit(solution)/shard_map/ppermute | solution.py:58
  1684.2 5.2 collective-permute-start.10
  1689.4 30.9 %collective-permute-done.10 = f32[3,256,512]{2,1,0:T(8,128)S(1)} collective-permute-done((f32[3,256,512]{2,1,0:T(8,128)S(1)}, f32[3,256,512]{2,1,0:T(8,128)S(1)}, u32[]{:S(2)}, u32[]{:S(2)}) %collective-permute-start.10) | collective-permute-done | bytes 1572896 | tf_op jit(solution)/shard_map/ppermute | solution.py:58
  1721.4 5.2 collective-permute-start.11
  1726.6 30.1 %collective-permute-done.11 = f32[3,256,512]{2,1,0:T(8,128)S(1)} collective-permute-done((f32[3,256,512]{2,1,0:T(8,128)S(1)}, f32[3,256,512]{2,1,0:T(8,128)S(1)}, u32[]{:S(2)}, u32[]{:S(2)}) %collective-permute-start.11) | collective-permute-done | bytes 1572896 | tf_op jit(solution)/shard_map/ppermute | solution.py:58
  1757.8 5.2 collective-permute-start.12
  1763.0 29.2 %collective-permute-done.12 = f32[3,256,512]{2,1,0:T(8,128)} collective-permute-done((f32[3,256,512]{2,1,0:T(8,128)S(1)}, f32[3,256,512]{2,1,0:T(8,128)}, u32[]{:S(2)}, u32[]{:S(2)}) %collective-permute-start.12) | collective-permute-done | bytes 1572896 | tf_op jit(solution)/shard_map/ppermute | solution.py:58
  1792.2 5.5 collective-permute-start.13
  1814.3 12.1 collective-permute-done.13
  1826.4 5.1 multiply_add_fusion.2
  1831.5 47.4 %all-gather.26.cloned.1.call-done = f32[3,256,2048]{2,1,0:T(8,128)} async-done(((f32[3,256,512]{2,1,0:T(8,128)}), f32[3,256,2048]{2,1,0:T(8,128)}) %all-gather.26.cloned.1.call-update) | async-done | bytes 6291472 | tf_op jit(solution)/shard_map/all_gather | solution.py:69
  1878.9 7.3 fusion.6
  1886.3 27.4 convolution_add_fusion.1
  1913.9 45.2 %all-gather.38.cloned.1.call-done = f32[2048,512]{1,0:T(8,128)} async-done(((f32[256,512]{1,0:T(8,128)}), f32[2048,512]{1,0:T(8,128)}) %all-gather.38.cloned.1.call-update) | async-done | bytes 4194320 | tf_op jit(solution)/shard_map/all_gather | solution.py:36
  1959.2 7.3 convolution_bitcast_fusion
  1966.5 434.3 %all-gather.28.cloned.1.call-done = f32[2,2048,1408]{2,1,0:T(8,128)} async-done(((f32[2,256,1408]{2,1,0:T(8,128)}), f32[2,2048,1408]{2,1,0:T(8,128)}) %all-gather.28.cloned.1.call-update) | async-done | bytes 23068688 | tf_op jit(solution)/shard_map/all_gather | solution.py:35
  2400.8 24.5 fusion.79
  2428.6 58.0 %reduce-scatter.8.cloned.1.call-done = f32[3,256,512]{2,1,0:T(8,128)} async-done(((f32[3,256,2048]{2,1,0:T(8,128)}), f32[3,256,512]{2,1,0:T(8,128)}) %reduce-scatter.8.cloned.1.call-update) | async-done | bytes 1572880 | tf_op jit(solution)/shard_map/reduce_scatter | solution.py:44
  2490.8 33.7 %collective-permute-done.14 = f32[3,256,512]{2,1,0:T(8,128)} collective-permute-done((f32[3,256,512]{2,1,0:T(8,128)}, f32[3,256,512]{2,1,0:T(8,128)}, u32[]{:S(2)}, u32[]{:S(2)}) %collective-permute-start.14) | collective-permute-done | bytes 1572896 | tf_op jit(solution)/shard_map/ppermute | solution.py:58
  2524.6 5.2 collective-permute-start.15
  2529.7 32.9 %collective-permute-done.15 = f32[3,256,512]{2,1,0:T(8,128)S(1)} collective-permute-done((f32[3,256,512]{2,1,0:T(8,128)}, f32[3,256,512]{2,1,0:T(8,128)S(1)}, u32[]{:S(2)}, u32[]{:S(2)}) %collective-permute-start.15) | collective-permute-done | bytes 1572896 | tf_op jit(solution)/shard_map/ppermute | solution.py:58
  2563.8 5.1 collective-permute-start.16
  2568.9 31.8 %collective-permute-done.16 = f32[3,256,512]{2,1,0:T(8,128)S(1)} collective-permute-done((f32[3,256,512]{2,1,0:T(8,128)S(1)}, f32[3,256,512]{2,1,0:T(8,128)S(1)}, u32[]{:S(2)}, u32[]{:S(2)}) %collective-permute-start.16) | collective-permute-done | bytes 1572896 | tf_op jit(solution)/shard_map/ppermute | solution.py:58
  2601.8 5.2 collective-permute-start.17
  2607.0 30.9 %collective-permute-done.17 = f32[3,256,512]{2,1,0:T(8,128)S(1)} collective-permute-done((f32[3,256,512]{2,1,0:T(8,128)S(1)}, f32[3,256,512]{2,1,0:T(8,128)S(1)}, u32[]{:S(2)}, u32[]{:S(2)}) %collective-permute-start.17) | collective-permute-done | bytes 1572896 | tf_op jit(solution)/shard_map/ppermute | solution.py:58
  2639.1 5.2 collective-permute-start.18
  2644.3 30.1 %collective-permute-done.18 = f32[3,256,512]{2,1,0:T(8,128)S(1)} collective-permute-done((f32[3,256,512]{2,1,0:T(8,128)S(1)}, f32[3,256,512]{2,1,0:T(8,128)S(1)}, u32[]{:S(2)}, u32[]{:S(2)}) %collective-permute-start.18) | collective-permute-done | bytes 1572896 | tf_op jit(solution)/shard_map/ppermute | solution.py:58
  2675.5 5.2 collective-permute-start.19
  2680.6 29.2 %collective-permute-done.19 = f32[3,256,512]{2,1,0:T(8,128)} collective-permute-done((f32[3,256,512]{2,1,0:T(8,128)S(1)}, f32[3,256,512]{2,1,0:T(8,128)}, u32[]{:S(2)}, u32[]{:S(2)}) %collective-permute-start.19) | collective-permute-done | bytes 1572896 | tf_op jit(solution)/shard_map/ppermute | solution.py:58
  2709.8 5.5 collective-permute-start.20
  2731.9 12.1 collective-permute-done.20
  2744.0 4.9 multiply_add_fusion.1
  2748.9 47.4 %all-gather.32.cloned.1.call-done = f32[3,256,2048]{2,1,0:T(8,128)} async-done(((f32[3,256,512]{2,1,0:T(8,128)}), f32[3,256,2048]{2,1,0:T(8,128)}) %all-gather.32.cloned.1.call-update) | async-done | bytes 6291472 | tf_op jit(solution)/shard_map/all_gather | solution.py:69
  2796.4 7.8 broadcast_multiply_fusion.1
  2804.2 35.0 %broadcast_multiply_fusion = (f32[2,256,1408]{2,1,0:T(8,128)}, f32[2,256,1408]{2,1,0:T(8,128)}) fusion(f32[2,256,1408]{2,1,0:T(8,128)} %param.6, f32[3,256,2048]{2,1,0:T(8,128)S(1)} %copy-done.35, f32[2,2048,1408]{2,1,0:T(8,128)} %all-gather.28.cloned.1.call-done, f32[2,256,1408]{2,1,0:T(8,128)S(1)} %copy-done.2), kind=kOutput, calls=%fused_computation.22 | convolution fusion | flops 17720344576 | bytes 40894464 | tf_op jit(solution)/shard_map/krs,ksc->krc/dot_general | solution.py:71
  (141 shorter events, 100.6 us)
Async XLA Ops:
  7.2 79.1 %all-gather.34.cloned.1.call-start = ((), (), s32[]{:S(2)}) async-start(), calls=%async_computation.15 | async-start | bytes 4718592 | tf_op jit(solution)/shard_map/all_gather | solution.py:36
  9.9 518.0 %all-gather.16.cloned.1.call-start = ((), (), s32[]{:S(2)}) async-start(), calls=%async_computation.3 | async-start | bytes 25952256 | tf_op jit(solution)/shard_map/all_gather | solution.py:35
  14.6 71.6 %copy-start.11 = (f32[256,512]{1,0:T(8,128)S(1)}, f32[256,512]{1,0:T(8,128)}, u32[]{:S(2)}) copy-start(f32[256,512]{1,0:T(8,128)} %get-tuple-element.11) | copy-start | bytes 1572868
  14.6 599.1 %reduce-scatter.4.cloned.1.call-start = ((), (), s32[]{:S(2)}) async-start(), calls=%async_computation.4 | async-start | bytes 7864320 | tf_op jit(solution)/shard_map/reduce_scatter | solution.py:44
  86.2 441.7 %copy-start = (f32[2,256,1408]{2,1,0:T(8,128)S(1)}, f32[2,256,1408]{2,1,0:T(8,128)}, u32[]{:S(2)}) copy-start(f32[2,256,1408]{2,1,0:T(8,128)} %get-tuple-element.9) | copy-start | bytes 8650756
  528.0 24.6 copy-start.8
  555.7 314.2 %all-gather.18.cloned.1.call-start = ((), (), s32[]{:S(2)}) async-start(), calls=%async_computation.5 | async-start | bytes 7864320 | tf_op jit(solution)/shard_map/all_gather | solution.py:45
  613.7 346.7 %all-gather.20.cloned.1.call-start = ((), (), s32[]{:S(2)}) async-start(), calls=%async_computation.6 | async-start | bytes 7864320 | tf_op jit(solution)/shard_map/all_gather | solution.py:69
  613.8 38.1 %collective-permute-start = (f32[3,256,512]{2,1,0:T(8,128)}, f32[3,256,512]{2,1,0:T(8,128)S(1)}, u32[]{:S(2)}, u32[]{:S(2)}) collective-permute-start(f32[3,256,512]{2,1,0:T(8,128)} %reduce-scatter.4.cloned.1.call-done), channel_id=1, source_target_pairs={{0,28},{4,0},{8,4},{12,8},{16,12},{20,16},{24,20},{28,24},{1,29},{... | collective-permute-start | bytes 4718600 | tf_op jit(solution)/shard_map/ppermute | solution.py:58
  651.9 75.8 %copy-start.16 = (f32[3,256,512]{2,1,0:T(8,128)}, f32[3,256,512]{2,1,0:T(8,128)S(1)}, u32[]{:S(2)}) copy-start(f32[3,256,512]{2,1,0:T(8,128)S(1)} %collective-permute-done) | copy-start | bytes 4718596
  651.9 37.7 %collective-permute-start.1 = (f32[3,256,512]{2,1,0:T(8,128)S(1)}, f32[3,256,512]{2,1,0:T(8,128)S(1)}, u32[]{:S(2)}, u32[]{:S(2)}) collective-permute-start(f32[3,256,512]{2,1,0:T(8,128)S(1)} %collective-permute-done), channel_id=1, source_target_pairs={{0,28},{4,0},{8,4},{12,8},{16,12},{20,16},{24,20},{28,24},{1,29},{... | collective-permute-start | bytes 4718600 | tf_op jit(solution)/shard_map/ppermute | solution.py:58
  690.7 37.0 %collective-permute-start.2 = (f32[3,256,512]{2,1,0:T(8,128)S(1)}, f32[3,256,512]{2,1,0:T(8,128)S(1)}, u32[]{:S(2)}, u32[]{:S(2)}) collective-permute-start(f32[3,256,512]{2,1,0:T(8,128)S(1)} %collective-permute-done.1), channel_id=1, source_target_pairs={{0,28},{4,0},{8,4},{12,8},{16,12},{20,16},{24,20},{28,24},{1,29},{... | collective-permute-start | bytes 4718600 | tf_op jit(solution)/shard_map/ppermute | solution.py:58
  727.7 5.2 copy-start.17
  727.7 36.1 %collective-permute-start.3 = (f32[3,256,512]{2,1,0:T(8,128)S(1)}, f32[3,256,512]{2,1,0:T(8,128)S(1)}, u32[]{:S(2)}, u32[]{:S(2)}) collective-permute-start(f32[3,256,512]{2,1,0:T(8,128)S(1)} %collective-permute-done.2), channel_id=1, source_target_pairs={{0,28},{4,0},{8,4},{12,8},{16,12},{20,16},{24,20},{28,24},{1,29},{... | collective-permute-start | bytes 4718600 | tf_op jit(solution)/shard_map/ppermute | solution.py:58
  764.9 35.2 %collective-permute-start.4 = (f32[3,256,512]{2,1,0:T(8,128)S(1)}, f32[3,256,512]{2,1,0:T(8,128)}, u32[]{:S(2)}, u32[]{:S(2)}) collective-permute-start(f32[3,256,512]{2,1,0:T(8,128)S(1)} %collective-permute-done.3), channel_id=1, source_target_pairs={{0,28},{4,0},{8,4},{12,8},{16,12},{20,16},{24,20},{28,24},{1,29},{... | collective-permute-start | bytes 4718600 | tf_op jit(solution)/shard_map/ppermute | solution.py:58
  800.2 73.1 %collective-permute-start.5 = (f32[3,256,512]{2,1,0:T(8,128)}, f32[3,256,512]{2,1,0:T(8,128)}, u32[]{:S(2)}, u32[]{:S(2)}) collective-permute-start(f32[3,256,512]{2,1,0:T(8,128)} %collective-permute-done.4), channel_id=1, source_target_pairs={{0,28},{4,0},{8,4},{12,8},{16,12},{20,16},{24,20},{28,24},{1,29},{... | collective-permute-start | bytes 4718600 | tf_op jit(solution)/shard_map/ppermute | solution.py:58
  870.0 9.8 copy-start.12
  873.3 6.5 copy-start.18
  873.3 35.6 %collective-permute-start.6 = (f32[3,256,512]{2,1,0:T(8,128)}, f32[3,256,512]{2,1,0:T(8,128)S(1)}, u32[]{:S(2)}, u32[]{:S(2)}) collective-permute-start(f32[3,256,512]{2,1,0:T(8,128)} %collective-permute-done.5), channel_id=1, source_target_pairs={{0,28},{4,0},{8,4},{12,8},{16,12},{20,16},{24,20},{28,24},{1,29},{... | collective-permute-start | bytes 4718600 | tf_op jit(solution)/shard_map/ppermute | solution.py:58
  879.8 1.5 copy-start.20
  882.9 3.1 copy-start.3
  912.2 129.1 %all-gather.36.cloned.1.call-start = ((), (), s32[]{:S(2)}) async-start(), calls=%async_computation.16 | async-start | bytes 4718592 | tf_op jit(solution)/shard_map/all_gather | solution.py:36
  968.4 514.7 %all-gather.22.cloned.1.call-start = ((), (), s32[]{:S(2)}) async-start(), calls=%async_computation.7 | async-start | bytes 25952256 | tf_op jit(solution)/shard_map/all_gather | solution.py:35
  995.9 45.5 %copy-start.7 = (f32[256,512]{1,0:T(8,128)S(1)}, f32[256,512]{1,0:T(8,128)}, u32[]{:S(2)}) copy-start(f32[256,512]{1,0:T(8,128)} %fusion.5) | copy-start | bytes 1572868
  995.9 572.9 %reduce-scatter.6.cloned.1.call-start = ((), (), s32[]{:S(2)}) async-start(), calls=%async_computation.8 | async-start | bytes 7864320 | tf_op jit(solution)/shard_map/reduce_scatter | solution.py:44
  1041.4 441.7 %copy-start.1 = (f32[2,256,1408]{2,1,0:T(8,128)S(1)}, f32[2,256,1408]{2,1,0:T(8,128)}, u32[]{:S(2)}) copy-start(f32[2,256,1408]{2,1,0:T(8,128)} %fusion) | copy-start | bytes 8650756
  1483.1 24.6 copy-start.9
  1510.9 286.8 %all-gather.24.cloned.1.call-start = ((), (), s32[]{:S(2)}) async-start(), calls=%async_computation.9 | async-start | bytes 7864320 | tf_op jit(solution)/shard_map/all_gather | solution.py:45
  1568.9 38.0 %collective-permute-start.7 = (f32[3,256,512]{2,1,0:T(8,128)}, f32[3,256,512]{2,1,0:T(8,128)}, u32[]{:S(2)}, u32[]{:S(2)}) collective-permute-start(f32[3,256,512]{2,1,0:T(8,128)} %reduce-scatter.6.cloned.1.call-done), channel_id=1, source_target_pairs={{0,28},{4,0},{8,4},{12,8},{16,12},{20,16},{24,20},{28,24},{1,29},{... | collective-permute-start | bytes 4718600 | tf_op jit(solution)/shard_map/ppermute | solution.py:58
  1573.1 305.8 %all-gather.26.cloned.1.call-start = ((), (), s32[]{:S(2)}) async-start(), calls=%async_computation.10 | async-start | bytes 7864320 | tf_op jit(solution)/shard_map/all_gather | solution.py:69
  1606.9 38.1 %collective-permute-start.8 = (f32[3,256,512]{2,1,0:T(8,128)}, f32[3,256,512]{2,1,0:T(8,128)S(1)}, u32[]{:S(2)}, u32[]{:S(2)}) collective-permute-start(f32[3,256,512]{2,1,0:T(8,128)} %collective-permute-done.7), channel_id=1, source_target_pairs={{0,28},{4,0},{8,4},{12,8},{16,12},{20,16},{24,20},{28,24},{1,29},{... | collective-permute-start | bytes 4718600 | tf_op jit(solution)/shard_map/ppermute | solution.py:58
  1646.2 36.9 %collective-permute-start.9 = (f32[3,256,512]{2,1,0:T(8,128)S(1)}, f32[3,256,512]{2,1,0:T(8,128)S(1)}, u32[]{:S(2)}, u32[]{:S(2)}) collective-permute-start(f32[3,256,512]{2,1,0:T(8,128)S(1)} %collective-permute-done.8), channel_id=1, source_target_pairs={{0,28},{4,0},{8,4},{12,8},{16,12},{20,16},{24,20},{28,24},{1,29},{... | collective-permute-start | bytes 4718600 | tf_op jit(solution)/shard_map/ppermute | solution.py:58
  1683.0 1.2 copy-start.25
  1684.2 36.1 %collective-permute-start.10 = (f32[3,256,512]{2,1,0:T(8,128)S(1)}, f32[3,256,512]{2,1,0:T(8,128)S(1)}, u32[]{:S(2)}, u32[]{:S(2)}) collective-permute-start(f32[3,256,512]{2,1,0:T(8,128)S(1)} %collective-permute-done.9), channel_id=1, source_target_pairs={{0,28},{4,0},{8,4},{12,8},{16,12},{20,16},{24,20},{28,24},{1,29},{... | collective-permute-start | bytes 4718600 | tf_op jit(solution)/shard_map/ppermute | solution.py:58
  1721.4 35.2 %collective-permute-start.11 = (f32[3,256,512]{2,1,0:T(8,128)S(1)}, f32[3,256,512]{2,1,0:T(8,128)S(1)}, u32[]{:S(2)}, u32[]{:S(2)}) collective-permute-start(f32[3,256,512]{2,1,0:T(8,128)S(1)} %collective-permute-done.10), channel_id=1, source_target_pairs={{0,28},{4,0},{8,4},{12,8},{16,12},{20,16},{24,20},{28,24},{1,29},{... | collective-permute-start | bytes 4718600 | tf_op jit(solution)/shard_map/ppermute | solution.py:58
  1757.8 34.4 %collective-permute-start.12 = (f32[3,256,512]{2,1,0:T(8,128)S(1)}, f32[3,256,512]{2,1,0:T(8,128)}, u32[]{:S(2)}, u32[]{:S(2)}) collective-permute-start(f32[3,256,512]{2,1,0:T(8,128)S(1)} %collective-permute-done.11), channel_id=1, source_target_pairs={{0,28},{4,0},{8,4},{12,8},{16,12},{20,16},{24,20},{28,24},{1,29},{... | collective-permute-start | bytes 4718600 | tf_op jit(solution)/shard_map/ppermute | solution.py:58
  1792.2 34.1 %collective-permute-start.13 = (f32[3,256,512]{2,1,0:T(8,128)}, f32[3,256,512]{2,1,0:T(8,128)}, u32[]{:S(2)}, u32[]{:S(2)}) collective-permute-start(f32[3,256,512]{2,1,0:T(8,128)} %collective-permute-done.12), channel_id=1, source_target_pairs={{0,28},{4,0},{8,4},{12,8},{16,12},{20,16},{24,20},{28,24},{1,29},{... | collective-permute-start | bytes 4718600 | tf_op jit(solution)/shard_map/ppermute | solution.py:58
  1797.7 3.3 copy-start.5
  1797.7 6.0 copy-start.14
  1803.7 3.1 copy-start.26
  1806.7 1.5 copy-start.32
  1808.3 1.5 copy-start.34
  1831.5 127.7 %all-gather.38.cloned.1.call-start = ((), (), s32[]{:S(2)}) async-start(), calls=%async_computation.17 | async-start | bytes 4718592 | tf_op jit(solution)/shard_map/all_gather | solution.py:36
  1886.2 514.5 %all-gather.28.cloned.1.call-start = ((), (), s32[]{:S(2)}) async-start(), calls=%async_computation.11 | async-start | bytes 25952256 | tf_op jit(solution)/shard_map/all_gather | solution.py:35
  1913.7 45.5 %copy-start.6 = (f32[256,512]{1,0:T(8,128)S(1)}, f32[256,512]{1,0:T(8,128)}, u32[]{:S(2)}) copy-start(f32[256,512]{1,0:T(8,128)} %fusion.6) | copy-start | bytes 1572868
  1913.7 572.8 %reduce-scatter.8.cloned.1.call-start = ((), (), s32[]{:S(2)}) async-start(), calls=%async_computation.12 | async-start | bytes 7864320 | tf_op jit(solution)/shard_map/reduce_scatter | solution.py:44
  1959.2 441.6 %copy-start.2 = (f32[2,256,1408]{2,1,0:T(8,128)S(1)}, f32[2,256,1408]{2,1,0:T(8,128)}, u32[]{:S(2)}) copy-start(f32[2,256,1408]{2,1,0:T(8,128)} %convolution_add_fusion.1) | copy-start | bytes 8650756
  2400.8 24.6 copy-start.10
  2428.5 286.8 %all-gather.30.cloned.1.call-start = ((), (), s32[]{:S(2)}) async-start(), calls=%async_computation.13 | async-start | bytes 7864320 | tf_op jit(solution)/shard_map/all_gather | solution.py:45
  2486.5 38.0 %collective-permute-start.14 = (f32[3,256,512]{2,1,0:T(8,128)}, f32[3,256,512]{2,1,0:T(8,128)}, u32[]{:S(2)}, u32[]{:S(2)}) collective-permute-start(f32[3,256,512]{2,1,0:T(8,128)} %reduce-scatter.8.cloned.1.call-done), channel_id=1, source_target_pairs={{0,28},{4,0},{8,4},{12,8},{16,12},{20,16},{24,20},{28,24},{1,29},{... | collective-permute-start | bytes 4718600 | tf_op jit(solution)/shard_map/ppermute | solution.py:58
  2490.8 305.6 %all-gather.32.cloned.1.call-start = ((), (), s32[]{:S(2)}) async-start(), calls=%async_computation.14 | async-start | bytes 7864320 | tf_op jit(solution)/shard_map/all_gather | solution.py:69
  2524.6 38.1 %collective-permute-start.15 = (f32[3,256,512]{2,1,0:T(8,128)}, f32[3,256,512]{2,1,0:T(8,128)S(1)}, u32[]{:S(2)}, u32[]{:S(2)}) collective-permute-start(f32[3,256,512]{2,1,0:T(8,128)} %collective-permute-done.14), channel_id=1, source_target_pairs={{0,28},{4,0},{8,4},{12,8},{16,12},{20,16},{24,20},{28,24},{1,29},{... | collective-permute-start | bytes 4718600 | tf_op jit(solution)/shard_map/ppermute | solution.py:58
  2563.8 36.8 %collective-permute-start.16 = (f32[3,256,512]{2,1,0:T(8,128)S(1)}, f32[3,256,512]{2,1,0:T(8,128)S(1)}, u32[]{:S(2)}, u32[]{:S(2)}) collective-permute-start(f32[3,256,512]{2,1,0:T(8,128)S(1)} %collective-permute-done.15), channel_id=1, source_target_pairs={{0,28},{4,0},{8,4},{12,8},{16,12},{20,16},{24,20},{28,24},{1,29},{... | collective-permute-start | bytes 4718600 | tf_op jit(solution)/shard_map/ppermute | solution.py:58
  2600.7 1.2 copy-start.23
  2601.8 36.1 %collective-permute-start.17 = (f32[3,256,512]{2,1,0:T(8,128)S(1)}, f32[3,256,512]{2,1,0:T(8,128)S(1)}, u32[]{:S(2)}, u32[]{:S(2)}) collective-permute-start(f32[3,256,512]{2,1,0:T(8,128)S(1)} %collective-permute-done.16), channel_id=1, source_target_pairs={{0,28},{4,0},{8,4},{12,8},{16,12},{20,16},{24,20},{28,24},{1,29},{... | collective-permute-start | bytes 4718600 | tf_op jit(solution)/shard_map/ppermute | solution.py:58
  2639.1 35.2 %collective-permute-start.18 = (f32[3,256,512]{2,1,0:T(8,128)S(1)}, f32[3,256,512]{2,1,0:T(8,128)S(1)}, u32[]{:S(2)}, u32[]{:S(2)}) collective-permute-start(f32[3,256,512]{2,1,0:T(8,128)S(1)} %collective-permute-done.17), channel_id=1, source_target_pairs={{0,28},{4,0},{8,4},{12,8},{16,12},{20,16},{24,20},{28,24},{1,29},{... | collective-permute-start | bytes 4718600 | tf_op jit(solution)/shard_map/ppermute | solution.py:58
  2675.5 34.4 %collective-permute-start.19 = (f32[3,256,512]{2,1,0:T(8,128)S(1)}, f32[3,256,512]{2,1,0:T(8,128)}, u32[]{:S(2)}, u32[]{:S(2)}) collective-permute-start(f32[3,256,512]{2,1,0:T(8,128)S(1)} %collective-permute-done.18), channel_id=1, source_target_pairs={{0,28},{4,0},{8,4},{12,8},{16,12},{20,16},{24,20},{28,24},{1,29},{... | collective-permute-start | bytes 4718600 | tf_op jit(solution)/shard_map/ppermute | solution.py:58
  2709.8 34.1 %collective-permute-start.20 = (f32[3,256,512]{2,1,0:T(8,128)}, f32[3,256,512]{2,1,0:T(8,128)}, u32[]{:S(2)}, u32[]{:S(2)}) collective-permute-start(f32[3,256,512]{2,1,0:T(8,128)} %collective-permute-done.19), channel_id=1, source_target_pairs={{0,28},{4,0},{8,4},{12,8},{16,12},{20,16},{24,20},{28,24},{1,29},{... | collective-permute-start | bytes 4718600 | tf_op jit(solution)/shard_map/ppermute | solution.py:58
  2715.3 3.3 copy-start.4
  2715.3 6.0 copy-start.13
  2721.3 3.1 copy-start.24
  2724.4 1.5 copy-start.28
  2725.9 1.5 copy-start.30
  2796.4 7.8 copy-start.35
  (8 other events, 9.2 us)
Sparse Core Ops, SparseCore 0:
  10.7 75.5 all-gather.33
  88.3 439.5 all-gather.15
  555.8 57.8 reduce-scatter.3
  615.1 46.3 all-gather.17
  912.3 48.0 all-gather.19
  968.5 72.7 all-gather.35
  1043.5 439.5 all-gather.21
  1511.0 57.8 reduce-scatter.5
  1573.2 43.5 all-gather.23
  1831.6 47.2 all-gather.25
  1886.4 72.7 all-gather.37
  1961.2 439.5 all-gather.27
  2428.6 57.8 reduce-scatter.7
  2490.9 43.3 all-gather.29
  2749.1 47.2 all-gather.31
